TPU v7x, 32 devices: a whole 2x2x4 slice. The times are simulated.
32 devices in a mesh: kv: 8 (over z, y), tp: 4 (over x, core).
Axes of the slice: x: 2, y: 2, z: 4, core: 2. Of those that a mesh axis runs over, the one named last changes fastest.
Arguments:
- tokens: bfloat16 [48, 24, 4096], P(None, None, 'kv'), may hold values from -6 to 6
- norm_gain: bfloat16 [4096], P('kv'), may hold values from 0.099609375 to 1.8984375
- w_query: bfloat16 [4096, 2048], P('kv', 'tp'), may hold values from -0.09375 to 0.09375
- w_key: bfloat16 [4096, 512], P('kv', 'tp'), may hold values from -0.09375 to 0.09375
- w_value: bfloat16 [4096, 512], P('kv', 'tp'), may hold values from -0.09375 to 0.09375
- w_forget: bfloat16 [4096, 32], replicated, may hold values from -0.09375 to 0.09375
- forget_bias: float32 [32], P('tp'), may hold values from -1 to 3
- query_gain: bfloat16 [64], replicated, may hold values from 0.099609375 to 1.8984375
- key_gain: bfloat16 [64], replicated, may hold values from 0.099609375 to 1.8984375
- w_out: bfloat16 [2048, 4096], P('tp', 'kv'), may hold values from -0.5 to 0.5
- key_cache: bfloat16 [48, 512, 8192], P(None, 'tp', 'kv'), may hold values from -46 to 46
- value_cache: bfloat16 [48, 512, 8192], P(None, 'tp', 'kv'), may hold values from -6 to 6
- gate_sums: float32 [48, 32, 8192], P(None, 'tp', 'kv'), may hold values from -1027 to 0, as said below
- parents: int32 [48, 24], replicated, may hold values from -1 to 22, as said below
- lengths: int32 [48], replicated, may hold values from 4096 to 8186
- accepted: int32 [48], replicated, may hold values from 0 to 6
Outputs:
- mixed: bfloat16 [48, 24, 4096], P(None, None, 'kv')
Inputs may be any that keep to these rules, and one draw needn't show every extreme that they name: `gate_sums`: for each sequence and head it never rises along the positions. `parents`: the parent of proposal i is -1 (the cache's last visible position) or one of the proposals i - 3 to i - 1. The accepted proposals stand in the cache right after the first lengths positions.
All inputs are finite; a program needn't handle non-finite values.
Results may differ from a plain program's by a relative error of at most 0.03.
Values may be sent and summed in bfloat16 or wider, within the bound.
A program may use at most 128 MiB of HBM per device.

v0:
```python
import functools

import jax
import jax.numpy as jnp
from jax import lax
from jax.experimental import pallas as pl
from jax.experimental.pallas import tpu as pltpu
from jax.sharding import PartitionSpec as P

eps = 1e-05
floor_value = -1e30
MESH = pl.DeviceIdType.MESH
NT = (((1,), (1,)), ((), ()))
HIGHEST = lax.Precision.HIGHEST


def greet(axis, size, me):
    barrier = pltpu.get_barrier_semaphore()
    for step in range(1, size):
        pl.semaphore_signal(
            barrier, inc=1, device_id={axis: lax.rem(me + step, size)}, device_id_type=MESH
        )
    pl.semaphore_wait(barrier, size - 1)


def move_kernel(axis, size, count, spread, *refs):
    sources, targets = refs[:count], refs[count : 2 * count]
    send_sem, recv_sem, own_sem = refs[2 * count :]
    me = lax.axis_index(axis)

    def piece(source, index):
        return source.at[index] if spread else source

    own = [
        pltpu.make_async_copy(piece(source, me), target.at[me], own_sem.at[k])
        for k, (source, target) in enumerate(zip(sources, targets))
    ]
    for copy in own:
        copy.start()
    greet(axis, size, me)
    copies = []
    for step in range(1, size):
        peer = lax.rem(me + step, size)
        for k, (source, target) in enumerate(zip(sources, targets)):
            copy = pltpu.make_async_remote_copy(
                src_ref=piece(source, peer),
                dst_ref=target.at[me],
                send_sem=send_sem.at[k, step - 1],
                recv_sem=recv_sem.at[k, step - 1],
                device_id={axis: peer},
                device_id_type=MESH,
            )
            copy.start()
            copies.append(copy)
    for copy in own:
        copy.wait()
    for copy in copies:
        copy.wait()


def move(axis, arrays, spread, ident):
    size = lax.axis_size(axis)
    count = len(arrays)
    shapes = [
        jax.ShapeDtypeStruct(a.shape if spread else (size, *a.shape), a.dtype) for a in arrays
    ]
    return pl.pallas_call(
        functools.partial(move_kernel, axis, size, count, spread),
        out_shape=shapes,
        in_specs=[pl.BlockSpec(memory_space=pl.ANY)] * count,
        out_specs=[pl.BlockSpec(memory_space=pl.ANY)] * count,
        scratch_shapes=[
            pltpu.SemaphoreType.DMA((count, size - 1)),
            pltpu.SemaphoreType.DMA((count, size - 1)),
            pltpu.SemaphoreType.DMA((count,)),
        ],
        compiler_params=pltpu.CompilerParams(collective_id=ident, has_side_effects=True),
        name=f"move{ident}",
    )(*arrays)


def lanes(rows):
    return lax.broadcasted_iota(jnp.int32, (rows, 128), 1)


def paired_norm(block, gain, low):
    squares = block * block
    first = jnp.sum(jnp.where(low, squares, 0.0), axis=1, keepdims=True)
    second = jnp.sum(jnp.where(low, 0.0, squares), axis=1, keepdims=True)
    mean_sq = jnp.where(low, first, second) * (1.0 / 64)
    return block * lax.rsqrt(mean_sq + eps) * gain


def finish_kernel(size, model_width, rounds, groups, sides, parts, parent, params, q_out, o_out, s_out):
    rows = q_out.shape[0]
    width = groups * 128
    lane = lanes(rows)
    low = lane < 64

    def total_of(start):
        piece = parts[0, :, start : start + 128].astype(jnp.float32)
        for j in range(1, size):
            piece = piece + parts[j, :, start : start + 128].astype(jnp.float32)
        return piece

    gate = total_of(width + 256)
    heads = sides * groups
    squares = jnp.sum(
        jnp.where((lane == heads) | (lane == heads + 1), gate, 0.0), axis=1, keepdims=True
    )
    inverse = lax.rsqrt(squares * (1.0 / model_width) + eps)
    query = []
    for g in range(groups):
        normed = paired_norm(total_of(128 * g) * inverse, params[0:1, :], low).astype(jnp.bfloat16)
        q_out[:, 128 * g : 128 * g + 128] = normed
        query.append(normed.astype(jnp.float32))
    keys = paired_norm(total_of(width) * inverse, params[1:2, :], low).astype(jnp.bfloat16)
    values = (total_of(width + 128) * inverse).astype(jnp.bfloat16)
    pre = jnp.where(lane < heads, gate * inverse + params[2:3, :], 0.0)
    log_gate = jnp.minimum(pre, 0.0) - jnp.log1p(jnp.exp(-jnp.abs(pre)))
    row_id = lax.broadcasted_iota(jnp.int32, (rows, rows), 0)
    col_id = lax.broadcasted_iota(jnp.int32, (rows, rows), 1)
    reach = jnp.where((col_id == row_id) | (col_id == parent[...]), 1.0, 0.0)
    for _ in range(rounds):
        half = reach.astype(jnp.bfloat16)
        reach = jnp.minimum(jnp.dot(half, half, preferred_element_type=jnp.float32), 1.0)
    path = jnp.dot(reach, log_gate, precision=HIGHEST, preferred_element_type=jnp.float32)
    pick = jnp.where(lanes(8) == lax.broadcasted_iota(jnp.int32, (8, 128), 0), 1.0, 0.0)
    path_t = lax.dot_general(pick, path, NT, precision=HIGHEST, preferred_element_type=jnp.float32)
    stats = jnp.zeros((rows, 128), jnp.float32)
    for g in range(groups):
        outs = []
        for side in range(sides):
            h = side * groups + g
            mine = low if side == 0 else lane >= 64
            q = jnp.where(mine, query[g] * 0.125, 0.0).astype(jnp.bfloat16)
            logits = lax.dot_general(q, keys, NT, preferred_element_type=jnp.float32)
            logits = jnp.where(reach > 0.5, logits - path_t[h : h + 1, :], floor_value)
            top = jnp.max(logits, axis=1, keepdims=True)
            weights = jnp.exp(logits - top)
            total = jnp.sum(weights, axis=1, keepdims=True)
            out = jnp.dot(weights.astype(jnp.bfloat16), values, preferred_element_type=jnp.float32)
            outs.append(out / total)
            stats = jnp.where(lane == h, top, jnp.where(lane == heads + h, total, stats))
        o_out[:, 128 * g : 128 * g + 128] = jnp.where(low, outs[0], outs[-1])
    s_out[...] = stats


def attend_kernel(batch, groups, sides, drafts, valid_ref, q_ref, k_ref, v_ref, g_ref, o_ref, s_ref):
    positions = k_ref.shape[2]
    heads = sides * groups
    base = lax.axis_index("kv") * positions
    lane = lanes(drafts)
    low = lane < 64
    place = lax.broadcasted_iota(jnp.int32, (heads, positions), 1)
    for b in range(batch):
        valid = valid_ref[pl.program_id(0) * batch + b] - base
        gates = g_ref[b]
        last = jnp.sum(jnp.where(place == valid - 1, gates, 0.0), axis=1, keepdims=True)
        gates = jnp.where(place < valid, gates, -floor_value)
        query = q_ref[b].astype(jnp.float32) * 0.125
        pieces = [query[:, 128 * g : 128 * g + 128] for g in range(groups)]
        if sides == 2:
            pieces = [jnp.where(low, p, 0.0) for p in pieces] + [
                jnp.where(low, 0.0, p) for p in pieces
            ]
        else:
            pieces = [p[:, :64] for p in pieces]
        wide = jnp.concatenate(pieces, axis=0).astype(jnp.bfloat16)
        logits = jnp.dot(wide, k_ref[b], preferred_element_type=jnp.float32)
        logits = logits.reshape(heads, drafts, positions) - gates[:, None, :]
        top = jnp.max(logits, axis=2, keepdims=True)
        weights = jnp.exp(logits - top)
        total = jnp.sum(weights, axis=2, keepdims=True)
        flat = weights.reshape(heads * drafts, positions).astype(jnp.bfloat16)
        out = lax.dot_general(flat, v_ref[b], NT, preferred_element_type=jnp.float32)
        if sides == 1:
            out = jnp.concatenate([out, jnp.zeros_like(out)], axis=1)
        out = out.reshape(heads, drafts, 128) / total
        stats = jnp.zeros((drafts, 128), jnp.float32)
        for h in range(heads):
            stats = jnp.where(lane == h, top[h], stats)
            stats = jnp.where(lane == heads + h, total[h], stats)
            stats = jnp.where(lane == 2 * heads + h, last[h : h + 1, :], stats)
        s_ref[b] = stats
        for g in range(groups):
            o_ref[b, :, 128 * g : 128 * g + 128] = jnp.where(
                low, out[g], out[(sides - 1) * groups + g]
            ).astype(jnp.bfloat16)


def merge_kernel(size, groups, sides, sums, stats, o_new, s_new, out):
    rows = out.shape[0]
    heads = sides * groups
    low = lanes(rows) < 64
    both = stats[0]
    for j in range(1, size):
        both = both + stats[j]
    last = pltpu.roll(both, 128 - 2 * heads, 1)
    tops = [stats[j] for j in range(size)] + [s_new[...] - last]
    totals = [pltpu.roll(stats[j], 128 - heads, 1) for j in range(size)]
    totals.append(pltpu.roll(s_new[...], 128 - heads, 1))
    top = functools.reduce(jnp.maximum, tops)
    shares = [jnp.exp(t - top) * n for t, n in zip(tops, totals)]
    norm = 1.0 / functools.reduce(jnp.add, shares)
    shares = [s * norm for s in shares]
    for g in range(groups):
        span = slice(128 * g, 128 * g + 128)
        acc = jnp.zeros((rows, 128), jnp.float32)
        for j, share in enumerate(shares):
            block = o_new[:, span] if j == size else sums[j, :, span].astype(jnp.float32)
            other = (sides - 1) * groups + g
            factor = jnp.where(low, share[:, g : g + 1], share[:, other : other + 1])
            acc = acc + factor * block
        out[:, span] = acc.astype(jnp.bfloat16)


def body(
    tokens,
    norm_gain,
    w_query,
    w_key,
    w_value,
    w_forget,
    forget_bias,
    query_gain,
    key_gain,
    w_out,
    key_cache,
    value_cache,
    gate_sums,
    parents,
    lengths,
    accepted,
):
    seq_count, drafts, local_width = tokens.shape
    row_count = seq_count * drafts
    head_dim = query_gain.shape[0]
    heads = forget_bias.shape[0]
    sides = w_key.shape[1] // head_dim
    groups = heads // sides
    positions = key_cache.shape[2]
    size, tp_size = lax.axis_size("kv"), lax.axis_size("tp")
    kv_index, tp_index = lax.axis_index("kv"), lax.axis_index("tp")
    model_width = local_width * size
    share = row_count // size
    query_width = 2 * groups * head_dim
    f32, bf16 = jnp.float32, jnp.bfloat16

    wide_rows = tokens.reshape(row_count, local_width).astype(f32)
    squares = jnp.sum(wide_rows * wide_rows, axis=1, keepdims=True)
    coarse = squares.astype(bf16).astype(f32)
    scaled = (wide_rows * norm_gain.astype(f32)[None, :]).astype(bf16)
    forget_rows = lax.dynamic_slice(
        w_forget, (kv_index * local_width, tp_index * heads), (local_width, heads)
    )
    w_pairs = w_query.reshape(local_width, sides, groups, head_dim).transpose(0, 2, 1, 3)
    w_pairs = jnp.pad(w_pairs, ((0, 0), (0, 0), (0, 2 - sides), (0, 0)))
    w_pairs = w_pairs.reshape(local_width, query_width)
    fill = ((0, 0), (0, 128 - sides * head_dim))
    w_all = jnp.concatenate(
        [w_pairs, jnp.pad(w_key, fill), jnp.pad(w_value, fill), jnp.pad(forget_rows, ((0, 0), (0, 128 - heads)))], axis=1
    )
    partial = jnp.dot(scaled, w_all, preferred_element_type=f32)
    column = jnp.arange(partial.shape[1])[None, :] - (query_width + 256)
    partial = jnp.where(
        column == heads, coarse, jnp.where(column == heads + 1, squares - coarse, partial)
    ).astype(bf16)
    (parts,) = move("kv", [partial.reshape(size, share, -1)], True, 0)

    params = jnp.stack(
        [
            jnp.tile(query_gain.astype(f32), 2),
            jnp.tile(key_gain.astype(f32), 2),
            jnp.pad(forget_bias, (0, 128 - heads)),
        ]
    )
    params = jnp.pad(params, ((0, 5), (0, 0)))
    seq_share = seq_count // size
    own_parents = lax.dynamic_slice(parents, (kv_index * seq_share, 0), (seq_share, drafts))
    starts = jnp.arange(seq_share, dtype=jnp.int32)[:, None] * drafts
    parent_rows = jnp.where(own_parents < 0, -1, own_parents + starts).reshape(share, 1)
    rounds = max(drafts - 1, 1).bit_length()
    query, o_new, s_new = pl.pallas_call(
        functools.partial(finish_kernel, size, model_width, rounds, groups, sides),
        out_shape=[
            jax.ShapeDtypeStruct((share, query_width), bf16),
            jax.ShapeDtypeStruct((share, query_width), f32),
            jax.ShapeDtypeStruct((share, 128), f32),
        ],
        name="finish",
    )(parts, parent_rows, params)
    (query_all,) = move("kv", [query], False, 1)

    batch = 4 if seq_count % 4 == 0 else 1
    valid = lengths + accepted
    by_seq = lambda i, *_: (i, 0, 0)
    weighted, stats = pl.pallas_call(
        functools.partial(attend_kernel, batch, groups, sides, drafts),
        out_shape=[
            jax.ShapeDtypeStruct((seq_count, drafts, query_width), bf16),
            jax.ShapeDtypeStruct((seq_count, drafts, 128), f32),
        ],
        grid_spec=pltpu.PrefetchScalarGridSpec(
            num_scalar_prefetch=1,
            grid=(seq_count // batch,),
            in_specs=[
                pl.BlockSpec((batch, drafts, query_width), by_seq),
                pl.BlockSpec((batch, key_cache.shape[1], positions), by_seq),
                pl.BlockSpec((batch, key_cache.shape[1], positions), by_seq),
                pl.BlockSpec((batch, heads, positions), by_seq),
            ],
            out_specs=[
                pl.BlockSpec((batch, drafts, query_width), by_seq),
                pl.BlockSpec((batch, drafts, 128), by_seq),
            ],
        ),
        name="attend",
    )(
        valid,
        query_all.reshape(seq_count, drafts, query_width),
        key_cache,
        value_cache,
        gate_sums,
    )
    sums, stats_all = move(
        "kv", [weighted.reshape(size, share, query_width), stats.reshape(size, share, 128)], True, 2
    )
    attended = pl.pallas_call(
        functools.partial(merge_kernel, size, groups, sides),
        out_shape=jax.ShapeDtypeStruct((share, query_width), bf16),
        name="merge",
    )(sums, stats_all, o_new, s_new)
    (attended,) = move("kv", [attended], False, 3)
    w_rows = w_out.reshape(sides, groups, head_dim, -1).transpose(1, 0, 2, 3)
    w_rows = jnp.pad(w_rows, ((0, 0), (0, 2 - sides), (0, 0), (0, 0))).reshape(query_width, -1)
    partial_out = jnp.dot(
        attended.reshape(row_count, query_width), w_rows, preferred_element_type=f32
    ).astype(bf16)
    (pieces,) = move("tp", [partial_out.reshape(tp_size, row_count // tp_size, -1)], True, 4)
    mixed = jnp.sum(pieces.astype(f32), axis=0).astype(bf16)
    (mixed,) = move("tp", [mixed], False, 5)
    return mixed.reshape(seq_count, drafts, local_width)


def solution(mesh):
    return jax.shard_map(
        body,
        mesh=mesh,
        in_specs=(
            P(None, None, "kv"),
            P("kv"),
            P("kv", "tp"),
            P("kv", "tp"),
            P("kv", "tp"),
            P(),
            P("tp"),
            P(),
            P(),
            P("tp", "kv"),
            P(None, "tp", "kv"),
            P(None, "tp", "kv"),
            P(None, "tp", "kv"),
            P(),
            P(),
            P(),
        ),
        out_specs=P(None, None, "kv"),
        check_vma=False,
    )
```

profile of v0, /device:TPU:21, one launch (start us, length us, event | category | flops | bytes accessed | tf_op | source)
XLA Modules:
  0.0 224.8 jit_solution(2060969850649389241)
XLA Ops:
  0.0 1.7 multiply_reduce_fusion
  1.8 0.7 convert_element_type.62
  2.5 0.2 fusion.2
  2.8 0.2 copy.25
  3.0 0.4 copy-done.3
  3.4 0.1 copy.27
  3.5 0.1 copy.28
  3.7 2.7 %fusion.1 = bf16[1152,896]{1,0:T(8,128)(2,1)} fusion(bf16[1152,512]{1,0:T(8,128)(2,1)S(1)} %fusion.2, bf16[1152]{0:T(1024)(128)(2,1)S(1)} %fusion.14, bf16[1152]{0:T(1024)(128)(2,1)S(1)} %convert_element_type.80, pred[896]{0:T(1024)(128)(4,1)S(1)} %get-tuple-element.19, pred[896]{0:T(1024)(128)(4,1)S(1)} %get-tuple-element.20, ...), kind=kOutput, calls=%fused_computation.2 | convolution fusion | flops 1063616512 | bytes 4045056 | tf_op jit(solution)/shard_map/dot_general | solution.py:264
  6.4 46.4 %move0.1.parts = bf16[8,144,896]{2,1,0:T(8,128)(2,1)} custom-call(bf16[8,144,896]{2,1,0:T(8,128)(2,1)} %bitcast.27), custom_call_target="tpu_custom_call" | custom-call | tf_op jit(solution)/shard_map/move0/pallas_call | solution.py:67
  53.1 0.7 reshape.89.parent
  53.8 0.1 stack_tile.6
  54.0 0.6 select_maximum_fusion.params
  54.6 4.4 %finish.1 = (bf16[144,512]{1,0:T(8,128)(2,1)}, f32[144,512]{1,0:T(8,128)}, f32[144,128]{1,0:T(8,128)}) custom-call(bf16[8,144,896]{2,1,0:T(8,128)(2,1)} %move0.1.parts, s32[144,1]{1,0:T(8,128)} %reshape.89.parent, f32[8,128]{1,0:T(8,128)} %select_maximum_fusion.params), custom_call_target="tpu_custom_call" | custom-call | tf_op jit(solution)/shard_map/finish/pallas_call | solution.py:284
  59.0 28.6 %move1.1 = bf16[8,144,512]{2,1,0:T(8,128)(2,1)} custom-call(bf16[144,512]{1,0:T(8,128)(2,1)} %get-tuple-element.12.refs_0_), custom_call_target="tpu_custom_call" | custom-call | tf_op jit(solution)/shard_map/move1/pallas_call | solution.py:67
  87.7 0.5 add.35.valid_ref
  88.2 23.0 %attend.1 = (bf16[48,24,512]{2,1,0:T(8,128)(2,1)}, f32[48,24,128]{2,1,0:T(8,128)}) custom-call(s32[48]{0:T(128)} %add.35.valid_ref, bf16[48,24,512]{2,1,0:T(8,128)(2,1)} %bitcast.24, bf16[48,128,1024]{2,1,0:T(8,128)(2,1)} %k_ref.1, bf16[48,128,1024]{2,1,0:T(8,128)(2,1)} %v_ref.1, f32[48,8,1024]{2,1,0:T(8,128)} %g_ref.1), custom_call_target="tpu_custom_call" | custom-call | tf_op jit(solution)/shard_map/attend/pallas_call | solution.py:298
  111.2 41.2 %move2.1 = (bf16[8,144,512]{2,1,0:T(8,128)(2,1)}, f32[8,144,128]{2,1,0:T(8,128)}) custom-call(bf16[8,144,512]{2,1,0:T(8,128)(2,1)} %bitcast.28, f32[8,144,128]{2,1,0:T(8,128)} %bitcast.31), custom_call_target="tpu_custom_call" | custom-call | tf_op jit(solution)/shard_map/move2/pallas_call | solution.py:67
  152.4 4.1 %merge.1.refs_0_ = bf16[144,512]{1,0:T(8,128)(2,1)} custom-call(bf16[8,144,512]{2,1,0:T(8,128)(2,1)} %get-tuple-element.15.sums, f32[8,144,128]{2,1,0:T(8,128)} %get-tuple-element.16.stats, f32[144,512]{1,0:T(8,128)} %get-tuple-element.17.o_new, f32[144,128]{1,0:T(8,128)} %get-tuple-element.18.s_new), custom_call_target="tpu_custom_call" | custom-call | tf_op jit(solution)/shard_map/merge/pallas_call | solution.py:329
  156.5 28.5 %move3.1 = bf16[8,144,512]{2,1,0:T(8,128)(2,1)} custom-call(bf16[144,512]{1,0:T(8,128)(2,1)} %merge.1.refs_0_), custom_call_target="tpu_custom_call" | custom-call | tf_op jit(solution)/shard_map/move3/pallas_call | solution.py:67
  185.1 3.1 %convolution_convert_fusion = bf16[1152,512]{1,0:T(8,128)(2,1)} fusion(bf16[1152,512]{1,0:T(8,128)(2,1)} %bitcast.30, bf16[512,512]{1,0:T(8,128)(2,1)S(1)} %bitcast.34), kind=kOutput, calls=%fused_computation.3 | convolution fusion | flops 604569600 | bytes 2883584 | tf_op jit(solution)/shard_map/dot_general | solution.py:337
  188.1 16.6 %move4.1 = bf16[4,288,512]{2,1,0:T(8,128)(2,1)} custom-call(bf16[4,288,512]{2,1,0:T(8,128)(2,1)} %bitcast.29), custom_call_target="tpu_custom_call" | custom-call | tf_op jit(solution)/shard_map/move4/pallas_call | solution.py:67
  204.8 2.2 reduce_sum.25.refs_0_
  207.0 15.4 %move5.1 = bf16[4,288,512]{2,1,0:T(8,128)(2,1)} custom-call(bf16[288,512]{1,0:T(8,128)(2,1)} %reduce_sum.25.refs_0_), custom_call_target="tpu_custom_call" | custom-call | tf_op jit(solution)/shard_map/move5/pallas_call | solution.py:67
  222.5 2.4 %copy.33 = bf16[48,24,512]{2,1,0:T(8,128)(2,1)} copy(bf16[48,24,512]{2,1,0:T(8,128)(2,1)} %bitcast.25) | data formatting | bytes 2359296
  (36 shorter events, 0.5 us)
Async XLA Ops:
  0.0 2.5 %copy-start = (bf16[48,24,512]{2,1,0:T(8,128)(2,1)S(1)}, bf16[48,24,512]{2,1,0:T(8,128)(2,1)}, u32[]{:S(2)}) copy-start(bf16[48,24,512]{2,1,0:T(8,128)(2,1)} %param.16) | copy-start | bytes 3538948
  0.0 2.7 %copy-start.1 = (bf16[512,512]{1,0:T(8,128)(2,1)S(1)}, bf16[512,512]{1,0:T(8,128)(2,1)}, u32[]{:S(2)}) copy-start(bf16[512,512]{1,0:T(8,128)(2,1)} %param.18) | copy-start | bytes 1572868
  2.5 0.9 copy-start.3
  2.5 1.0 copy-start.4
  2.8 0.9 dynamic-slice-start
  6.4 46.5 %copy-start.5 = (s32[48,24]{0,1:T(8,128)S(1)}, s32[48,24]{0,1:T(8,128)}, u32[]{:S(2)}) copy-start(s32[48,24]{0,1:T(8,128)} %param.29) | copy-start | bytes 13828
  6.4 47.4 %copy-start.6 = (bf16[64]{0:T(256)(128)(2,1)S(1)}, bf16[64]{0:T(256)(128)(2,1)}, u32[]{:S(2)}) copy-start(bf16[64]{0:T(256)(128)(2,1)} %param.23) | copy-start | bytes 388
  6.4 47.5 %copy-start.7 = (bf16[64]{0:T(256)(128)(2,1)S(1)}, bf16[64]{0:T(256)(128)(2,1)}, u32[]{:S(2)}) copy-start(bf16[64]{0:T(256)(128)(2,1)} %param.24) | copy-start | bytes 388
  6.4 47.6 %copy-start.8 = (f32[8]{0:T(128)S(1)}, f32[8]{0:T(128)}, u32[]{:S(2)}) copy-start(f32[8]{0:T(128)} %param.22) | copy-start | bytes 100
  52.9 34.8 %copy-start.9 = (s32[48]{0:T(128)S(1)}, s32[48]{0:T(128)}, u32[]{:S(2)}) copy-start(s32[48]{0:T(128)} %param.30) | copy-start | bytes 580
  52.9 34.8 %copy-start.10 = (s32[48]{0:T(128)S(1)}, s32[48]{0:T(128)}, u32[]{:S(2)}) copy-start(s32[48]{0:T(128)} %param.31) | copy-start | bytes 580
  152.4 32.7 %copy-start.2 = (bf16[512,512]{1,0:T(8,128)(2,1)S(1)}, bf16[512,512]{1,0:T(8,128)(2,1)}, u32[]{:S(2)}) copy-start(bf16[512,512]{1,0:T(8,128)(2,1)} %param.25) | copy-start | bytes 1572868
where the time goes:
time: 228 us; the launch traced here: 225 us
  Pallas kernels  208 us (91%)
  other arithmetic  6.07 us (3%)
  matrix products  5.79 us (3%)
  local copies, waits for them, and re-layouts  4.38 us (2%)
    pallas_call x6, Pallas kernels, move(): pl.pallas_call(functools.partial(move_kernel, axis, size, count, spread),...  177 us
    pallas_call x1, Pallas kernels, body(): pl.pallas_call(functools.partial(attend_kernel, batch, groups, sides, dra...  23 us

commit v1 on v0

--- a/solution.py
+++ b/solution.py
@@ -23,16 +23,13 @@
     pl.semaphore_wait(barrier, size - 1)
 
 
-def move_kernel(axis, size, count, spread, *refs):
+def move_kernel(axis, size, count, *refs):
     sources, targets = refs[:count], refs[count : 2 * count]
     send_sem, recv_sem, own_sem = refs[2 * count :]
     me = lax.axis_index(axis)
 
-    def piece(source, index):
-        return source.at[index] if spread else source
-
     own = [
-        pltpu.make_async_copy(piece(source, me), target.at[me], own_sem.at[k])
+        pltpu.make_async_copy(source.at[me], target.at[me], own_sem.at[k])
         for k, (source, target) in enumerate(zip(sources, targets))
     ]
     for copy in own:
@@ -43,7 +40,7 @@
         peer = lax.rem(me + step, size)
         for k, (source, target) in enumerate(zip(sources, targets)):
             copy = pltpu.make_async_remote_copy(
-                src_ref=piece(source, peer),
+                src_ref=source.at[peer],
                 dst_ref=target.at[me],
                 send_sem=send_sem.at[k, step - 1],
                 recv_sem=recv_sem.at[k, step - 1],
@@ -58,14 +55,12 @@
         copy.wait()
 
 
-def move(axis, arrays, spread, ident):
+def move(axis, arrays, ident):
     size = lax.axis_size(axis)
     count = len(arrays)
-    shapes = [
-        jax.ShapeDtypeStruct(a.shape if spread else (size, *a.shape), a.dtype) for a in arrays
-    ]
+    shapes = [jax.ShapeDtypeStruct(a.shape, a.dtype) for a in arrays]
     return pl.pallas_call(
-        functools.partial(move_kernel, axis, size, count, spread),
+        functools.partial(move_kernel, axis, size, count),
         out_shape=shapes,
         in_specs=[pl.BlockSpec(memory_space=pl.ANY)] * count,
         out_specs=[pl.BlockSpec(memory_space=pl.ANY)] * count,
@@ -77,6 +72,64 @@
         compiler_params=pltpu.CompilerParams(collective_id=ident, has_side_effects=True),
         name=f"move{ident}",
     )(*arrays)
+
+
+def gather_kernel(axis, size, source, target, pair_send, pair_recv, far_send, far_recv, own_sem):
+    me = lax.axis_index(axis)
+    partner = me + 1 - 2 * lax.rem(me, 2)
+    half = size // 2
+    column = [lax.rem(me + 2 * step, size) for step in range(1, half)]
+    own = pltpu.make_async_copy(source, target.at[me], own_sem)
+    own.start()
+    barrier = pltpu.get_barrier_semaphore()
+    for peer in [partner] + column:
+        pl.semaphore_signal(barrier, inc=1, device_id={axis: peer}, device_id_type=MESH)
+    pl.semaphore_wait(barrier, half)
+
+    def send(block, slot, sems, index, peer):
+        copy = pltpu.make_async_remote_copy(
+            src_ref=block,
+            dst_ref=target.at[slot],
+            send_sem=sems[0].at[index],
+            recv_sem=sems[1].at[index],
+            device_id={axis: peer},
+            device_id_type=MESH,
+        )
+        copy.start()
+        return copy
+
+    near_sems, far_sems = (pair_send, pair_recv), (far_send, far_recv)
+    far = [send(source, me, far_sems, k, peer) for k, peer in enumerate(column)]
+    near = [send(source, me, near_sems, 0, partner)]
+    for k, copy in enumerate(far):
+        copy.wait_recv()
+        origin = lax.rem(me + size - 2 * (k + 1), size)
+        near.append(send(target.at[origin], origin, near_sems, k + 1, partner))
+    own.wait()
+    for copy in far:
+        copy.wait_send()
+    for copy in near:
+        copy.wait()
+
+
+def gather(axis, array, ident):
+    size = lax.axis_size(axis)
+    half = size // 2
+    return pl.pallas_call(
+        functools.partial(gather_kernel, axis, size),
+        out_shape=jax.ShapeDtypeStruct((size, *array.shape), array.dtype),
+        in_specs=[pl.BlockSpec(memory_space=pl.ANY)],
+        out_specs=pl.BlockSpec(memory_space=pl.ANY),
+        scratch_shapes=[
+            pltpu.SemaphoreType.DMA((half,)),
+            pltpu.SemaphoreType.DMA((half,)),
+            pltpu.SemaphoreType.DMA((half - 1,)),
+            pltpu.SemaphoreType.DMA((half - 1,)),
+            pltpu.SemaphoreType.DMA,
+        ],
+        compiler_params=pltpu.CompilerParams(collective_id=ident, has_side_effects=True),
+        name=f"gather{ident}",
+    )(array)
 
 
 def lanes(rows):
@@ -266,7 +319,7 @@
     partial = jnp.where(
         column == heads, coarse, jnp.where(column == heads + 1, squares - coarse, partial)
     ).astype(bf16)
-    (parts,) = move("kv", [partial.reshape(size, share, -1)], True, 0)
+    (parts,) = move("kv", [partial.reshape(size, share, -1)], 0)
 
     params = jnp.stack(
         [
@@ -290,7 +343,7 @@
         ],
         name="finish",
     )(parts, parent_rows, params)
-    (query_all,) = move("kv", [query], False, 1)
+    query_all = gather("kv", query, 1)
 
     batch = 4 if seq_count % 4 == 0 else 1
     valid = lengths + accepted
@@ -324,22 +377,22 @@
         gate_sums,
     )
     sums, stats_all = move(
-        "kv", [weighted.reshape(size, share, query_width), stats.reshape(size, share, 128)], True, 2
+        "kv", [weighted.reshape(size, share, query_width), stats.reshape(size, share, 128)], 2
     )
     attended = pl.pallas_call(
         functools.partial(merge_kernel, size, groups, sides),
         out_shape=jax.ShapeDtypeStruct((share, query_width), bf16),
         name="merge",
     )(sums, stats_all, o_new, s_new)
-    (attended,) = move("kv", [attended], False, 3)
+    attended = gather("kv", attended, 3)
     w_rows = w_out.reshape(sides, groups, head_dim, -1).transpose(1, 0, 2, 3)
     w_rows = jnp.pad(w_rows, ((0, 0), (0, 2 - sides), (0, 0), (0, 0))).reshape(query_width, -1)
     partial_out = jnp.dot(
         attended.reshape(row_count, query_width), w_rows, preferred_element_type=f32
     ).astype(bf16)
-    (pieces,) = move("tp", [partial_out.reshape(tp_size, row_count // tp_size, -1)], True, 4)
+    (pieces,) = move("tp", [partial_out.reshape(tp_size, row_count // tp_size, -1)], 4)
     mixed = jnp.sum(pieces.astype(f32), axis=0).astype(bf16)
-    (mixed,) = move("tp", [mixed], False, 5)
+    mixed = gather("tp", mixed, 5)
     return mixed.reshape(seq_count, drafts, local_width)
 
 

time: 228 us -> 212 us (0.930); the launches traced: 225 us -> 212 us
  Pallas kernels: 208 us -> 195 us
    pallas_call x6, Pallas kernels: 177 us -> 164 us  [the longest x3 112 us: move(): pl.pallas_call(functools.partial(move_kernel, axis, size, count), out_sha...]
where the time goes in v1:
time: 212 us
  Pallas kernels  195 us (92%)
  other arithmetic  6.07 us (3%)
  matrix products  5.8 us (3%)
  local copies, waits for them, and re-layouts  4.38 us (2%)
    pallas_call x3, Pallas kernels, move(): pl.pallas_call(functools.partial(move_kernel, axis, size, count), out_sha...  112 us
    pallas_call x3, Pallas kernels, gather(): pl.pallas_call(functools.partial(gather_kernel, axis, size), out_shape=ja...  52.1 us
    pallas_call x1, Pallas kernels, body(): pl.pallas_call(functools.partial(attend_kernel, batch, groups, sides, dra...  23 us
    pallas_call x1, Pallas kernels, body(): pl.pallas_call(functools.partial(finish_kernel, size, model_width, rounds...  4.44 us

profile of v1, /device:TPU:21, one launch (start us, length us, event | category | flops | bytes accessed | tf_op | source)
XLA Modules:
  0.0 211.7 jit_solution(1288716210459908904)
XLA Ops:
  0.0 1.7 multiply_reduce_fusion
  1.8 0.7 convert_element_type.62
  2.5 0.2 fusion.2
  2.8 0.2 copy.25
  3.0 0.4 copy-done.3
  3.4 0.1 copy.27
  3.5 0.1 copy.28
  3.7 2.7 %fusion.1 = bf16[1152,896]{1,0:T(8,128)(2,1)} fusion(bf16[1152,512]{1,0:T(8,128)(2,1)S(1)} %fusion.2, bf16[1152]{0:T(1024)(128)(2,1)S(1)} %fusion.14, bf16[1152]{0:T(1024)(128)(2,1)S(1)} %convert_element_type.80, pred[896]{0:T(1024)(128)(4,1)S(1)} %get-tuple-element.19, pred[896]{0:T(1024)(128)(4,1)S(1)} %get-tuple-element.20, ...), kind=kOutput, calls=%fused_computation.2 | convolution fusion | flops 1063616512 | bytes 4045056 | tf_op jit(solution)/shard_map/dot_general | solution.py:317
  6.4 46.4 %move0.1.parts = bf16[8,144,896]{2,1,0:T(8,128)(2,1)} custom-call(bf16[8,144,896]{2,1,0:T(8,128)(2,1)} %bitcast.27), custom_call_target="tpu_custom_call" | custom-call | tf_op jit(solution)/shard_map/move0/pallas_call | solution.py:62
  53.1 0.7 reshape.89.parent
  53.8 0.1 stack_tile.6
  54.0 0.6 select_maximum_fusion.params
  54.6 4.4 %finish.1 = (bf16[144,512]{1,0:T(8,128)(2,1)}, f32[144,512]{1,0:T(8,128)}, f32[144,128]{1,0:T(8,128)}) custom-call(bf16[8,144,896]{2,1,0:T(8,128)(2,1)} %move0.1.parts, s32[144,1]{1,0:T(8,128)} %reshape.89.parent, f32[8,128]{1,0:T(8,128)} %select_maximum_fusion.params), custom_call_target="tpu_custom_call" | custom-call | tf_op jit(solution)/shard_map/finish/pallas_call | solution.py:337
  59.0 17.0 %gather1.1 = bf16[8,144,512]{2,1,0:T(8,128)(2,1)} custom-call(bf16[144,512]{1,0:T(8,128)(2,1)} %get-tuple-element.12.source), custom_call_target="tpu_custom_call" | custom-call | tf_op jit(solution)/shard_map/gather1/pallas_call | solution.py:118
  76.1 0.5 add.35.valid_ref
  76.6 23.0 %attend.1 = (bf16[48,24,512]{2,1,0:T(8,128)(2,1)}, f32[48,24,128]{2,1,0:T(8,128)}) custom-call(s32[48]{0:T(128)} %add.35.valid_ref, bf16[48,24,512]{2,1,0:T(8,128)(2,1)} %bitcast.24, bf16[48,128,1024]{2,1,0:T(8,128)(2,1)} %k_ref.1, bf16[48,128,1024]{2,1,0:T(8,128)(2,1)} %v_ref.1, f32[48,8,1024]{2,1,0:T(8,128)} %g_ref.1), custom_call_target="tpu_custom_call" | custom-call | tf_op jit(solution)/shard_map/attend/pallas_call | solution.py:351
  99.6 47.2 %move2.1 = (bf16[8,144,512]{2,1,0:T(8,128)(2,1)}, f32[8,144,128]{2,1,0:T(8,128)}) custom-call(bf16[8,144,512]{2,1,0:T(8,128)(2,1)} %bitcast.28, f32[8,144,128]{2,1,0:T(8,128)} %bitcast.31), custom_call_target="tpu_custom_call" | custom-call | tf_op jit(solution)/shard_map/move2/pallas_call | solution.py:62
  146.8 4.1 %merge.1.source = bf16[144,512]{1,0:T(8,128)(2,1)} custom-call(bf16[8,144,512]{2,1,0:T(8,128)(2,1)} %get-tuple-element.15.sums, f32[8,144,128]{2,1,0:T(8,128)} %get-tuple-element.16.stats, f32[144,512]{1,0:T(8,128)} %get-tuple-element.17.o_new, f32[144,128]{1,0:T(8,128)} %get-tuple-element.18.s_new), custom_call_target="tpu_custom_call" | custom-call | tf_op jit(solution)/shard_map/merge/pallas_call | solution.py:382
  150.9 23.8 %gather3.1 = bf16[8,144,512]{2,1,0:T(8,128)(2,1)} custom-call(bf16[144,512]{1,0:T(8,128)(2,1)} %merge.1.source), custom_call_target="tpu_custom_call" | custom-call | tf_op jit(solution)/shard_map/gather3/pallas_call | solution.py:118
  174.8 3.1 %convolution_convert_fusion = bf16[1152,512]{1,0:T(8,128)(2,1)} fusion(bf16[1152,512]{1,0:T(8,128)(2,1)} %bitcast.30, bf16[512,512]{1,0:T(8,128)(2,1)S(1)} %bitcast.34), kind=kOutput, calls=%fused_computation.3 | convolution fusion | flops 604569600 | bytes 2883584 | tf_op jit(solution)/shard_map/dot_general | solution.py:390
  177.9 18.0 %move4.1 = bf16[4,288,512]{2,1,0:T(8,128)(2,1)} custom-call(bf16[4,288,512]{2,1,0:T(8,128)(2,1)} %bitcast.29), custom_call_target="tpu_custom_call" | custom-call | tf_op jit(solution)/shard_map/move4/pallas_call | solution.py:62
  195.9 2.2 %reduce_sum.25.source = bf16[288,512]{1,0:T(8,128)(2,1)} reduce(bf16[4,288,512]{2,1,0:T(8,128)(2,1)} %move4.1, bf16[]{:T(256)} %constant.35.clone.1), dimensions={0}, to_apply=%region_1.2 | reduce | flops 442368 | bytes 1474562 | tf_op jit(solution)/shard_map/reduce_sum | solution.py:394
  198.1 11.2 %gather5.1 = bf16[4,288,512]{2,1,0:T(8,128)(2,1)} custom-call(bf16[288,512]{1,0:T(8,128)(2,1)} %reduce_sum.25.source), custom_call_target="tpu_custom_call" | custom-call | tf_op jit(solution)/shard_map/gather5/pallas_call | solution.py:118
  209.4 2.4 %copy.33 = bf16[48,24,512]{2,1,0:T(8,128)(2,1)} copy(bf16[48,24,512]{2,1,0:T(8,128)(2,1)} %bitcast.25) | data formatting | bytes 2359296
  (36 shorter events, 0.5 us)
Async XLA Ops:
  0.0 2.5 %copy-start = (bf16[48,24,512]{2,1,0:T(8,128)(2,1)S(1)}, bf16[48,24,512]{2,1,0:T(8,128)(2,1)}, u32[]{:S(2)}) copy-start(bf16[48,24,512]{2,1,0:T(8,128)(2,1)} %param.16) | copy-start | bytes 3538948
  0.0 2.7 %copy-start.1 = (bf16[512,512]{1,0:T(8,128)(2,1)S(1)}, bf16[512,512]{1,0:T(8,128)(2,1)}, u32[]{:S(2)}) copy-start(bf16[512,512]{1,0:T(8,128)(2,1)} %param.18) | copy-start | bytes 1572868
  2.5 0.9 copy-start.3
  2.5 1.0 copy-start.4
  2.8 0.9 dynamic-slice-start
  6.4 46.5 %copy-start.5 = (s32[48,24]{0,1:T(8,128)S(1)}, s32[48,24]{0,1:T(8,128)}, u32[]{:S(2)}) copy-start(s32[48,24]{0,1:T(8,128)} %param.29) | copy-start | bytes 13828
  6.4 47.4 %copy-start.6 = (bf16[64]{0:T(256)(128)(2,1)S(1)}, bf16[64]{0:T(256)(128)(2,1)}, u32[]{:S(2)}) copy-start(bf16[64]{0:T(256)(128)(2,1)} %param.23) | copy-start | bytes 388
  6.4 47.5 %copy-start.7 = (bf16[64]{0:T(256)(128)(2,1)S(1)}, bf16[64]{0:T(256)(128)(2,1)}, u32[]{:S(2)}) copy-start(bf16[64]{0:T(256)(128)(2,1)} %param.24) | copy-start | bytes 388
  6.4 47.6 %copy-start.8 = (f32[8]{0:T(128)S(1)}, f32[8]{0:T(128)}, u32[]{:S(2)}) copy-start(f32[8]{0:T(128)} %param.22) | copy-start | bytes 100
  52.9 23.2 %copy-start.9 = (s32[48]{0:T(128)S(1)}, s32[48]{0:T(128)}, u32[]{:S(2)}) copy-start(s32[48]{0:T(128)} %param.30) | copy-start | bytes 580
  52.9 23.2 %copy-start.10 = (s32[48]{0:T(128)S(1)}, s32[48]{0:T(128)}, u32[]{:S(2)}) copy-start(s32[48]{0:T(128)} %param.31) | copy-start | bytes 580
  146.8 28.0 %copy-start.2 = (bf16[512,512]{1,0:T(8,128)(2,1)S(1)}, bf16[512,512]{1,0:T(8,128)(2,1)}, u32[]{:S(2)}) copy-start(bf16[512,512]{1,0:T(8,128)(2,1)} %param.25) | copy-start | bytes 1572868
